TPU v7x, 32 devices: a whole 2x2x4 slice. The times are simulated.
32 devices in a mesh: grp: 2 (over x), tp: 4 (over z), dp: 4 (over y, core).
Axes of the slice: x: 2, y: 2, z: 4, core: 2. Of those that a mesh axis runs over, the one named last changes fastest.
Arguments:
- tokens: bfloat16 [8, 4, 4096], P(('grp', 'tp'), None, 'dp'), parts along dimension 0, may hold values from -6 to 6
- lengths: int32 [8], P('grp'), parts along dimension 0, may hold values from 1 to 4, 8 in all
- norm_gain: float32 [2, 4096], P(None, 'dp'), may hold values from 0.1 to 1.9
- input_weight: bfloat16 [2, 4096, 8192], P(None, 'dp', 'tp'), may hold values from -0.09375 to 0.09375
- gate_weight: bfloat16 [2, 4096, 8192], P(None, 'dp', 'tp'), may hold values from -0.09375 to 0.09375
- decay_rate: float32 [2, 512, 64], P(None, 'tp'), may hold values from 0.05 to 2
- frequency: float32 [2, 512, 64], P(None, 'tp'), may hold values from 0 to 4
- log_step: float32 [2, 512], P(None, 'tp'), may hold values from -2.3 to 0
- input_map: bfloat16 [2, 512, 16, 128], P(None, 'tp'), may hold values from -1 to 1
- readout_map: bfloat16 [2, 512, 16, 128], P(None, 'tp'), may hold values from -0.5 to 0.5
- skip_weight: bfloat16 [2, 8192], P(None, 'tp'), may hold values from -4 to 4
- out_weight: bfloat16 [2, 8192, 4096], P(None, 'tp', 'dp'), may hold values from -0.0625 to 0.0625
- state: float32 [2, 8, 512, 128], P(None, ('grp', 'dp'), 'tp'), parts along dimension 1, may hold values from -5 to 5
Outputs:
- mixed: bfloat16 [8, 4, 4096], P(('grp', 'tp'), None, 'dp'), parts along dimension 0
- new_state: float32 [2, 8, 512, 128], P(None, ('grp', 'dp'), 'tp'), parts along dimension 1
There are 2 independent parts, one for each index of `grp`. A program takes and returns all parts, laid end to end along the dimension named above; an argument that names none is the same for every part. Nothing has to cross between parts.
Inputs may be any that keep to these rules, and one draw needn't show every extreme that they name: `lengths`: the number of live new positions of each sequence; positions beyond it take no part.
All inputs are finite; a program needn't handle non-finite values.
Results may differ from a plain program's by a relative error of at most 0.023.
Values may be sent and summed in bfloat16 or wider, within the bound.
A program may use at most 64 MiB of HBM per device.

v0:
```python
import jax
import jax.numpy as jnp
from jax import lax
from jax.sharding import PartitionSpec as P

D = 4096
S5_IN = 16
LAYERS = 2


epsilon = 1e-06


def advance_state(
    drive_value,
    gate_value,
    carried,
    alive_mask,
    decay_rate,
    frequency,
    log_step,
    input_map,
    readout_map,
    skip_row,
):
    seq_count, new_count, inner_width = drive_value.shape
    group_count = inner_width // S5_IN
    state_half = carried.shape[-1] // 2
    step_size = jnp.exp(log_step)[:, None]
    magnitude = jnp.exp(-decay_rate * step_size)
    turn_angle = frequency * step_size
    decay_real = magnitude * jnp.cos(turn_angle)
    decay_imag = magnitude * jnp.sin(turn_angle)
    denominator = decay_rate * decay_rate + frequency * frequency
    coeff_real = (-(decay_real - 1.0) * decay_rate + decay_imag * frequency) / denominator
    coeff_imag = (-decay_imag * decay_rate - (decay_real - 1.0) * frequency) / denominator
    map_real = input_map[..., :state_half].astype(jnp.float32)
    map_imag = input_map[..., state_half:].astype(jnp.float32)
    coupled = jnp.concatenate(
        [
            coeff_real[:, None, :] * map_real - coeff_imag[:, None, :] * map_imag,
            coeff_real[:, None, :] * map_imag + coeff_imag[:, None, :] * map_real,
        ],
        axis=-1,
    )
    inputs = drive_value.astype(jnp.float32).reshape(seq_count, new_count, group_count, S5_IN)
    pushed = jnp.einsum("stgi,giq->stgq", inputs, coupled, precision=lax.Precision.HIGHEST)
    real_state = carried[..., :state_half]
    imag_state = carried[..., state_half:]
    history = []
    for position in range(new_count):
        keep = alive_mask[:, position][:, None, None] > 0.5
        next_real = (
            decay_real * real_state - decay_imag * imag_state + pushed[:, position, :, :state_half]
        )
        next_imag = (
            decay_real * imag_state + decay_imag * real_state + pushed[:, position, :, state_half:]
        )
        real_state = jnp.where(keep, next_real, real_state)
        imag_state = jnp.where(keep, next_imag, imag_state)
        history.append(jnp.concatenate([real_state, -imag_state], axis=-1))
    stacked = jnp.stack(history, axis=1)
    readout = jnp.einsum(
        "stgq,giq->stgi", stacked, readout_map.astype(jnp.float32), precision=lax.Precision.HIGHEST
    )
    readout = readout.reshape(seq_count, new_count, inner_width)
    response = readout + skip_row.astype(jnp.float32) * inputs.reshape(
        seq_count, new_count, inner_width
    )
    branch = (
        jax.nn.gelu(response) * jax.nn.silu(gate_value.astype(jnp.float32)) * alive_mask[:, :, None]
    )
    return (jnp.concatenate([real_state, imag_state], axis=-1), branch.astype(jnp.bfloat16))


def body(
    tokens,
    lengths,
    norm_gain,
    input_weight,
    gate_weight,
    decay_rate,
    frequency,
    log_step,
    input_map,
    readout_map,
    skip_weight,
    out_weight,
    state,
):
    own_seqs = state.shape[1]
    block_seqs, new_count, feature_count = tokens.shape
    all_seqs = lengths.shape[0]
    inner_width = input_weight.shape[2]
    dp_index = lax.axis_index("dp")
    tp_index = lax.axis_index("tp")
    positions = lax.broadcasted_iota(jnp.int32, (all_seqs, new_count), 1)
    alive_all = (positions < lengths[:, None]).astype(jnp.float32)
    alive_own = lax.dynamic_slice_in_dim(alive_all, dp_index * own_seqs, own_seqs, 0)
    own_rows = own_seqs * new_count
    block_count = block_seqs * new_count
    own_block = tokens
    states = []
    for layer_index in range(LAYERS):
        gathered = lax.all_gather(own_block, "tp", axis=0, tiled=True)
        flattened = gathered.reshape(all_seqs * new_count, feature_count).astype(jnp.float32)
        scaled = (flattened * norm_gain[layer_index][None, :]).astype(jnp.bfloat16)
        partial_squares = jnp.sum(flattened * flattened, axis=1)
        part_drive = jnp.dot(scaled, input_weight[layer_index], preferred_element_type=jnp.float32)
        part_gate = jnp.dot(scaled, gate_weight[layer_index], preferred_element_type=jnp.float32)
        total_squares = lax.psum(partial_squares, "dp")
        summed_drive, summed_gate = (
            lax.psum_scatter(
                part_drive.astype(jnp.bfloat16), "dp", scatter_dimension=0, tiled=True
            ).astype(jnp.float32),
            lax.psum_scatter(
                part_gate.astype(jnp.bfloat16), "dp", scatter_dimension=0, tiled=True
            ).astype(jnp.float32),
        )
        own_squares = lax.dynamic_slice_in_dim(total_squares, dp_index * own_rows, own_rows, 0)
        inverse = lax.rsqrt(own_squares / D + epsilon)[:, None]
        drive_value = (
            (inverse * summed_drive).astype(jnp.bfloat16).reshape(own_seqs, new_count, inner_width)
        )
        gate_value = (
            (inverse * summed_gate).astype(jnp.bfloat16).reshape(own_seqs, new_count, inner_width)
        )
        next_state, branch = advance_state(
            drive_value,
            gate_value,
            state[layer_index],
            alive_own,
            decay_rate[layer_index],
            frequency[layer_index],
            log_step[layer_index],
            input_map[layer_index],
            readout_map[layer_index],
            skip_weight[layer_index],
        )
        states.append(next_state)
        weight_now = out_weight[layer_index]
        projected = jnp.dot(
            lax.all_gather(branch.reshape(own_rows, inner_width), "dp", axis=0, tiled=True),
            weight_now,
            preferred_element_type=jnp.float32,
        )
        branch_sum = lax.psum_scatter(
            projected.astype(jnp.bfloat16), "tp", scatter_dimension=0, tiled=True
        ).astype(jnp.float32)
        own_base = lax.dynamic_slice_in_dim(flattened, tp_index * block_count, block_count, 0)
        own_block = (own_base + branch_sum).astype(jnp.bfloat16).reshape(tokens.shape)
    return (own_block, jnp.stack(states))


def solution(mesh):
    return jax.shard_map(
        body,
        mesh=mesh,
        in_specs=(
            P(("grp", "tp"), None, "dp"),
            P("grp"),
            P(None, "dp"),
            P(None, "dp", "tp"),
            P(None, "dp", "tp"),
            P(None, "tp", None),
            P(None, "tp", None),
            P(None, "tp"),
            P(None, "tp", None, None),
            P(None, "tp", None, None),
            P(None, "tp"),
            P(None, "tp", "dp"),
            P(None, ("grp", "dp"), "tp", None),
        ),
        out_specs=(P(("grp", "tp"), None, "dp"), P(None, ("grp", "dp"), "tp", None)),
        check_vma=False,
    )
```

profile of v0, /device:TPU:0, one launch (start us, length us, event | category | flops | bytes accessed | tf_op | source)
XLA Modules:
  0.0 198.8 jit_solution(4493405564464504982)
XLA Ops:
  7.3 15.2 %all_gather.12 = bf16[4,4,1024]{2,1,0:T(4,128)(2,1)S(1)} all-gather(bf16[1,4,1024]{2,1,0:T(4,128)(2,1)} %param.13), channel_id=1, replica_groups=mesh['grp'=2,'tp'=4,'dp'=4] {'tp'}, dimensions={0}, use_global_device_ids=true | all-gather | bytes 40960 | tf_op jit(solution)/shard_map/all_gather | solution.py:105
  23.4 3.5 %fusion.21 = bf16[16,2048]{1,0:T(8,128)(2,1)} fusion(bf16[16,1024]{1,0:T(8,128)(2,1)S(1)} %convert_element_type.158, bf16[2,1024,2048]{2,1,0:T(8,128)(2,1)} %param.17), kind=kOutput, calls=%fused_computation.19 | convolution fusion | flops 67141632 | bytes 4292608 | tf_op jit(solution)/shard_map/dot_general | solution.py:110
  26.9 3.5 %fusion.18 = bf16[16,2048]{1,0:T(8,128)(2,1)} fusion(bf16[16,1024]{1,0:T(8,128)(2,1)S(1)} %convert_element_type.158, bf16[2,1024,2048]{2,1,0:T(8,128)(2,1)} %param.16), kind=kOutput, calls=%fused_computation.18 | convolution fusion | flops 67141632 | bytes 4292608 | tf_op jit(solution)/shard_map/dot_general | solution.py:109
  31.2 5.6 %psum.14 = f32[16]{0:T(128)S(1)} all-reduce(f32[16]{0:T(128)S(1)} %reduce_sum.23), channel_id=1, replica_groups=mesh['grp'=2,'tp'=4,'dp'=4] {'dp'}, use_global_device_ids=true, to_apply=%region_1.0 | all-reduce | flops 16 | bytes 128 | tf_op jit(solution)/shard_map/psum | solution.py:111
  43.7 1.7 fusion.36
  45.9 17.5 %all-reduce.13.cloned.1.call-done = (bf16[16,2048]{1,0:T(8,128)(2,1)}, bf16[16,2048]{1,0:T(8,128)(2,1)}) async-done(((bf16[16,2048]{1,0:T(8,128)(2,1)}, bf16[16,2048]{1,0:T(8,128)(2,1)}), (bf16[16,2048]{1,0:T(8,128)(2,1)}, bf16[16,2048]{1,0:T(8,128)(2,1)})) %all-reduce.13.cloned.1.call-update) | async-done | bytes 131088
  64.3 2.4 %fusion.40 = f32[128,128,4]{1,2,0:T(4,128)S(1)} fusion(f32[128,16,64]{2,1,0:T(8,128)} %get-tuple-element.37, f32[128,16,64]{2,1,0:T(8,128)} %get-tuple-element.36, bf16[4,128,16]{2,1,0:T(8,128)(2,1)S(1)} %reshape.438), kind=kOutput, calls=%fused_computation.38 | convolution fusion | flops 12845056 | bytes 1327104 | tf_op jit(solution)/shard_map/stgi,giq->stgq/dot_general | solution.py:47
  68.0 2.0 convolution_bitcast_fusion.1
  71.0 5.2 %all-gather.1 = bf16[4,4,2048]{2,1,0:T(4,128)(2,1)S(1)} all-gather(bf16[1,4,2048]{2,1,0:T(4,128)(2,1)S(1)} %fusion.127), channel_id=1, replica_groups=mesh['grp'=2,'tp'=4,'dp'=4] {'dp'}, dimensions={0}, use_global_device_ids=true | all-gather | bytes 81920 | tf_op jit(solution)/shard_map/all_gather | solution.py:143
  76.3 2.8 %fusion.30 = bf16[16,1024]{1,0:T(8,128)(2,1)S(1)} fusion(bf16[16,2048]{1,0:T(8,128)(2,1)S(1)} %reshape.456, bf16[2,2048,1024]{2,1,0:T(8,128)(2,1)} %param.24), kind=kOutput, calls=%fused_computation.32 | convolution fusion | flops 67125248 | bytes 4292608 | tf_op jit(solution)/shard_map/dot_general | solution.py:142
  79.1 19.1 %all-reduce.2 = bf16[16,1024]{1,0:T(8,128)(2,1)S(1)} all-reduce(bf16[16,1024]{1,0:T(8,128)(2,1)S(1)} %fusion.30), channel_id=5, replica_groups=mesh['grp'=2,'tp'=4,'dp'=4] {'tp'}, use_global_device_ids=true, to_apply=%region_4.5.clone | all-reduce | flops 16384 | bytes 65536
  99.0 13.1 %all-gather.2 = bf16[4,4,1024]{2,1,0:T(4,128)(2,1)S(1)} all-gather(bf16[1,4,1024]{2,1,0:T(4,128)(2,1)S(1)} %fusion.129), channel_id=2, replica_groups=mesh['grp'=2,'tp'=4,'dp'=4] {'tp'}, dimensions={0}, use_global_device_ids=true | all-gather | bytes 40960 | tf_op jit(solution)/shard_map/all_gather | solution.py:105
  112.9 3.5 %fusion.27 = bf16[16,2048]{1,0:T(8,128)(2,1)} fusion(bf16[16,1024]{1,0:T(8,128)(2,1)S(1)} %convert_element_type.179, bf16[2,1024,2048]{2,1,0:T(8,128)(2,1)} %param.17), kind=kOutput, calls=%fused_computation.21 | convolution fusion | flops 67141632 | bytes 4292608 | tf_op jit(solution)/shard_map/dot_general | solution.py:110
  116.4 3.5 %fusion.24 = bf16[16,2048]{1,0:T(8,128)(2,1)} fusion(bf16[16,1024]{1,0:T(8,128)(2,1)S(1)} %convert_element_type.179, bf16[2,1024,2048]{2,1,0:T(8,128)(2,1)} %param.16), kind=kOutput, calls=%fused_computation.20 | convolution fusion | flops 67141632 | bytes 4292608 | tf_op jit(solution)/shard_map/dot_general | solution.py:109
  120.0 5.9 %psum.15 = f32[16]{0:T(128)S(1)} all-reduce(f32[16]{0:T(128)S(1)} %reduce_sum.25), channel_id=1, replica_groups=mesh['grp'=2,'tp'=4,'dp'=4] {'dp'}, use_global_device_ids=true, to_apply=%region_6.7 | all-reduce | flops 16 | bytes 128 | tf_op jit(solution)/shard_map/psum | solution.py:111
  125.9 29.1 %all-reduce.11.cloned.1.call-done = (bf16[16,2048]{1,0:T(8,128)(2,1)}, bf16[16,2048]{1,0:T(8,128)(2,1)}) async-done(((bf16[16,2048]{1,0:T(8,128)(2,1)}, bf16[16,2048]{1,0:T(8,128)(2,1)}), (bf16[16,2048]{1,0:T(8,128)(2,1)}, bf16[16,2048]{1,0:T(8,128)(2,1)})) %all-reduce.11.cloned.1.call-update) | async-done | bytes 131088
  156.7 1.7 fusion.44
  158.6 0.9 fusion.134
  159.9 0.9 convolution_bitcast_fusion
  161.0 0.9 fusion.128
  161.9 5.2 %all-gather.3 = bf16[4,4,2048]{2,1,0:T(4,128)(2,1)S(1)} all-gather(bf16[1,4,2048]{2,1,0:T(4,128)(2,1)S(1)} %fusion.128), channel_id=1, replica_groups=mesh['grp'=2,'tp'=4,'dp'=4] {'dp'}, dimensions={0}, use_global_device_ids=true | all-gather | bytes 81920 | tf_op jit(solution)/shard_map/all_gather | solution.py:143
  167.2 2.8 %fusion.33 = bf16[16,1024]{1,0:T(8,128)(2,1)S(1)} fusion(bf16[16,2048]{1,0:T(8,128)(2,1)S(1)} %reshape.460, bf16[2,2048,1024]{2,1,0:T(8,128)(2,1)} %param.24), kind=kOutput, calls=%fused_computation.33 | convolution fusion | flops 67125248 | bytes 4292608 | tf_op jit(solution)/shard_map/dot_general | solution.py:142
  170.0 19.0 %all-reduce.5 = bf16[16,1024]{1,0:T(8,128)(2,1)S(1)} all-reduce(bf16[16,1024]{1,0:T(8,128)(2,1)S(1)} %fusion.33), channel_id=8, replica_groups=mesh['grp'=2,'tp'=4,'dp'=4] {'tp'}, use_global_device_ids=true, to_apply=%region_9.10.clone | all-reduce | flops 16384 | bytes 65536
  190.6 1.4 fusion.130
  (94 shorter events, 14.0 us)
Async XLA Ops:
  7.2 33.8 %copy-start.12 = (u32[32]{0:T(128)S(1)}, u32[32]{0:T(128)}, u32[]{:S(2)}) copy-start(u32[32]{0:T(128)} %constant.47) | copy-start | bytes 388
  7.2 34.3 %copy-start.11 = (u32[32]{0:T(128)S(1)}, u32[32]{0:T(128)}, u32[]{:S(2)}) copy-start(u32[32]{0:T(128)} %constant.55) | copy-start | bytes 388
  7.2 23.9 %copy-start.10 = (s32[4]{0:T(128)S(1)}, s32[4]{0:T(128)}, u32[]{:S(2)}) copy-start(s32[4]{0:T(128)} %param.14) | copy-start | bytes 52
  7.2 29.7 %copy-start.9 = (f32[2,128]{1,0:T(2,128)S(1)}, f32[2,128]{1,0:T(2,128)}, u32[]{:S(2)}) copy-start(f32[2,128]{1,0:T(2,128)} %param.20) | copy-start | bytes 3076
  7.2 29.7 %copy-start.2 = (f32[2,128,64]{1,2,0:T(8,128)S(1)}, f32[2,128,64]{1,2,0:T(8,128)}, u32[]{:S(2)}) copy-start(f32[2,128,64]{1,2,0:T(8,128)} %param.18) | copy-start | bytes 196612
  7.2 29.7 %copy-start.3 = (f32[2,128,64]{1,2,0:T(8,128)S(1)}, f32[2,128,64]{1,2,0:T(8,128)}, u32[]{:S(2)}) copy-start(f32[2,128,64]{1,2,0:T(8,128)} %param.19) | copy-start | bytes 196612
  7.2 30.2 %copy-start = (bf16[2,128,16,128]{3,2,1,0:T(8,128)(2,1)S(1)}, bf16[2,128,16,128]{3,2,1,0:T(8,128)(2,1)}, u32[]{:S(2)}) copy-start(bf16[2,128,16,128]{3,2,1,0:T(8,128)(2,1)} %param.21) | copy-start | bytes 3145732
  7.2 30.4 %copy-start.4 = (f32[2,1,128,128]{3,2,1,0:T(8,128)S(1)}, f32[2,1,128,128]{3,2,1,0:T(8,128)}, u32[]{:S(2)}) copy-start(f32[2,1,128,128]{3,2,1,0:T(8,128)} %param.25) | copy-start | bytes 393220
  7.3 33.6 %copy-start.5 = (bf16[2,2048]{1,0:T(2,128)(2,1)S(1)}, bf16[2,2048]{1,0:T(2,128)(2,1)}, u32[]{:S(2)}) copy-start(bf16[2,2048]{1,0:T(2,128)(2,1)} %param.23) | copy-start | bytes 24580
  7.3 56.1 %all-reduce.13.cloned.1.call-start = ((), (), s32[]{:S(2)}) async-start(), calls=%async_computation.1 | async-start | bytes 262144
  30.4 124.7 %all-reduce.11.cloned.1.call-start = ((), (), s32[]{:S(2)}) async-start(), calls=%async_computation | async-start | bytes 262144
  31.1 39.0 %copy-start.6 = (f32[4]{0:T(128)}, f32[4]{0:T(128)S(1)}, u32[]{:S(2)}) copy-start(f32[4]{0:T(128)S(1)} %fusion.163) | copy-start | bytes 52
  79.1 80.7 %copy-start.1 = (bf16[2,128,16,128]{3,2,1,0:T(8,128)(2,1)S(1)}, bf16[2,128,16,128]{3,2,1,0:T(8,128)(2,1)}, u32[]{:S(2)}) copy-start(bf16[2,128,16,128]{3,2,1,0:T(8,128)(2,1)} %param.22) | copy-start | bytes 3145732
  112.9 48.1 %copy-start.7 = (f32[4]{0:T(128)S(1)}, f32[4]{0:T(128)}, u32[]{:S(2)}) copy-start(f32[4]{0:T(128)} %copy-done.6) | copy-start | bytes 52
  125.9 30.8 %copy-start.8 = (f32[4]{0:T(128)}, f32[4]{0:T(128)S(1)}, u32[]{:S(2)}) copy-start(f32[4]{0:T(128)S(1)} %add_rsqrt_fusion) | copy-start | bytes 52
Sparse Core Ops, SparseCore 0:
  30.5 32.8 all-reduce.12
  126.0 29.0 all-reduce.10
where the time goes:
time: 200 us; the launch traced here: 199 us
  blocking collectives  88.4 us (44%)
  waiting for transfers between devices  46.7 us (23%)
  matrix products  26.6 us (13%)
  between operations  18.3 us (9%)
  other arithmetic  11.3 us (6%)
  local copies, waits for them, and re-layouts  7.52 us (4%)
    unnamed x4, waiting for transfers between devices  46.7 us
    unnamed x2, blocking collectives  38.1 us
    all_gather x2, blocking collectives, body(): gathered = lax.all_gather(own_block, 'tp', axis=0, tiled=True)  28.3 us
    psum x2, blocking collectives, body(): total_squares = lax.psum(partial_squares, 'dp')  11.5 us
    all_gather x2, blocking collectives, body(): lax.all_gather(branch.reshape(own_rows, inner_width), 'dp', axis=0, tiled...  10.5 us
    dot_general x2, matrix products, body(): jnp.dot(scaled, gate_weight[layer_index], preferred_element_type=jnp.floa...  6.96 us
    dot_general x2, matrix products, body(): jnp.dot(scaled, input_weight[layer_index], preferred_element_type=jnp.flo...  6.92 us
    dot_general x2, matrix products, body(): jnp.dot(lax.all_gather(branch.reshape(own_rows, inner_width), 'dp', axis=...  5.69 us
  transfers between devices with their start and end apart: 2, of which 2 were waited for; matrix products, arithmetic and copies ran while one was open for 3% of the time, Pallas kernels for 0%

commit v1 on v0

v1 whole, which is shorter than its diff:
```python
import functools

import jax
import jax.numpy as jnp
from jax import lax
from jax.experimental import pallas as pl
from jax.experimental.pallas import tpu as pltpu
from jax.sharding import PartitionSpec as P

D = 4096
S5_IN = 16
CHUNKS = 4
LANES = 128

epsilon = 1e-06
f32, bf16 = jnp.float32, jnp.bfloat16


def kernel(
    n_tp,
    n_dp,
    lengths,
    tokens,
    norm_gain,
    input_weight,
    gate_weight,
    decay_rate,
    frequency,
    log_step,
    input_map,
    readout_map,
    skip_weight,
    out_weight,
    state,
    mixed_out,
    state_out,
    v_gain,
    v_in,
    v_gate,
    v_decay,
    v_freq,
    v_step,
    v_imap,
    v_rmap,
    v_skip,
    v_out,
    v_state,
    v_mixed,
    x_recv,
    x_all,
    sq_send,
    sq_recv,
    part_send,
    part_recv,
    branch_all,
    b_rows,
    read_rows,
    tp_all,
    rs_send,
    rs_recv,
    coef,
    sem_small,
    sem_w,
    sem_out,
    sem_x,
    sem_sq,
    sem_part,
    sem_branch,
    sem_tp,
    sem_rs,
):
    layers, own_seqs, groups, state_width = state.shape
    block_rows, features = tokens.shape
    inner = input_weight.shape[2]
    width = inner // CHUNKS
    all_seqs = lengths.shape[0]
    new = block_rows * n_tp // all_seqs
    own_rows = own_seqs * new
    rows = all_seqs * new
    half = state_width // 2
    per_tile = LANES // S5_IN
    tiles = width // LANES
    tp_me = lax.axis_index("tp")
    dp_me = lax.axis_index("dp")

    def local(src, dst, sem):
        copy = pltpu.make_async_copy(src, dst, sem)
        copy.start()
        return copy

    small = [
        local(src, dst, sem_small.at[i])
        for i, (src, dst) in enumerate(
            (
                (tokens, x_recv.at[tp_me]),
                (norm_gain, v_gain),
                (decay_rate, v_decay),
                (frequency, v_freq),
                (log_step, v_step),
                (skip_weight, v_skip),
                (state, v_state),
            )
        )
    ]
    fetch = {}
    for l in range(layers):
        for n in range(CHUNKS):
            cols = pl.ds(n * width, width)
            fetch["in", l, n] = local(input_weight.at[l, :, cols], v_in.at[l, n], sem_w.at[l, n, 0])
            fetch["gate", l, n] = local(gate_weight.at[l, :, cols], v_gate.at[l, n], sem_w.at[l, n, 1])
        fetch["imap", l] = local(input_map.at[l], v_imap.at[l], sem_w.at[l, 0, 3])
        fetch["rmap", l] = local(readout_map.at[l], v_rmap.at[l], sem_w.at[l, 1, 3])
        for n in range(CHUNKS):
            cols = pl.ds(n * width, width)
            fetch["out", l, n] = local(out_weight.at[l, cols, :], v_out.at[l, n], sem_w.at[l, n, 2])

    barrier = pltpu.get_barrier_semaphore()
    tp_peers = [lax.rem(tp_me + k, n_tp) for k in range(1, n_tp)]
    dp_peers = [lax.rem(dp_me + k, n_dp) for k in range(1, n_dp)]
    for peer in tp_peers:
        pl.semaphore_signal(
            barrier, inc=1, device_id={"tp": peer}, device_id_type=pl.DeviceIdType.MESH
        )
    for peer in dp_peers:
        pl.semaphore_signal(
            barrier, inc=1, device_id={"dp": peer}, device_id_type=pl.DeviceIdType.MESH
        )
    pl.semaphore_wait(barrier, n_tp + n_dp - 2)

    sends = []

    def push(axis, peer, src, dst, sems):
        copy = pltpu.make_async_remote_copy(
            src_ref=src,
            dst_ref=dst,
            send_sem=sems.at[0],
            recv_sem=sems.at[1],
            device_id={axis: peer},
            device_id_type=pl.DeviceIdType.MESH,
        )
        copy.start()

    def settle(ref, sem):
        pltpu.make_async_copy(ref, ref, sem).wait()

    small[0].wait()
    for peer in tp_peers:
        push("tp", peer, x_recv.at[tp_me], x_recv.at[tp_me], sem_x)
    sends.append((x_recv.at[pl.ds(0, n_tp - 1)], sem_x.at[0]))

    for copy in small[1:]:
        copy.wait()
    for l in range(layers):
        step = jnp.exp(jnp.broadcast_to(v_step[l : l + 1, :], (LANES, groups)).T)[:, :half]
        rate = v_decay[l]
        freq = v_freq[l]
        magnitude = jnp.exp(-rate * step)
        angle = freq * step
        ar = magnitude * jnp.cos(angle)
        ai = magnitude * jnp.sin(angle)
        den = rate * rate + freq * freq
        cr = (-(ar - 1.0) * rate + ai * freq) / den
        ci = (-ai * rate - (ar - 1.0) * freq) / den
        for i, (low, high) in enumerate(((ar, ar), (-ai, ai), (cr, cr), (-ci, ci))):
            coef[l, i, :, 0:half] = low
            coef[l, i, :, half:] = high

    settle(x_recv.at[pl.ds(0, n_tp - 1)], sem_x.at[1])
    for j in range(n_tp):
        x_all[j * block_rows : (j + 1) * block_rows, :] = x_recv[j].astype(f32)
    x = x_all[...]

    lane = lax.broadcasted_iota(jnp.int32, (per_tile, LANES), 1)
    sub = lax.broadcasted_iota(jnp.int32, (per_tile, LANES), 0)
    own_group = (lane >= sub * S5_IN) & (lane < (sub + 1) * S5_IN)
    sign = jnp.where(
        lax.broadcasted_iota(jnp.int32, (1, state_width), 1) < half, jnp.float32(1), jnp.float32(-1)
    )
    lens = [lengths[dp_me * own_seqs + s] for s in range(own_seqs)]
    row_id = lax.broadcasted_iota(jnp.int32, (own_rows, 1), 0)
    alive = jnp.zeros((own_rows, 1), f32)
    for s in range(own_seqs):
        inside = (row_id >= s * new) & (row_id < s * new + lens[s])
        alive = jnp.where(inside, jnp.float32(1), alive)

    for l in range(layers):
        squares = jnp.sum(x * x, axis=1, keepdims=True)
        wide = jnp.broadcast_to(squares, (rows, LANES))
        for j in range(n_dp):
            sq_send[l, j] = wide[j * own_rows : (j + 1) * own_rows, :]
        for k, peer in enumerate(dp_peers):
            push("dp", peer, sq_send.at[l, peer], sq_recv.at[l, k], sem_sq.at[l])
        sends.append((sq_recv.at[l], sem_sq.at[l, 0]))
        scaled = (x * v_gain[l : l + 1, :]).astype(bf16)
        for n in range(CHUNKS):
            fetch["in", l, n].wait()
            drive_part = jnp.dot(scaled, v_in[l, n], preferred_element_type=f32)
            fetch["gate", l, n].wait()
            gate_part = jnp.dot(scaled, v_gate[l, n], preferred_element_type=f32)
            for j in range(n_dp):
                own = slice(j * own_rows, (j + 1) * own_rows)
                part_send[l, n, j, :, 0:width] = drive_part[own].astype(bf16)
                part_send[l, n, j, :, width:] = gate_part[own].astype(bf16)
            for k, peer in enumerate(dp_peers):
                push("dp", peer, part_send.at[l, n, peer], part_recv.at[l, n, k], sem_part.at[l, n])
            sends.append((part_recv.at[l, n], sem_part.at[l, n, 0]))

        fetch["imap", l].wait()
        fetch["rmap", l].wait()
        settle(sq_recv.at[l], sem_sq.at[l, 1])
        total = sq_send[l, dp_me]
        for k in range(n_dp - 1):
            total = total + sq_recv[l, k]
        inverse = lax.rsqrt(total[:, 0:1] / D + epsilon)
        skip_row = v_skip[...].astype(f32)[l : l + 1, :]
        for n in range(CHUNKS):
            settle(part_recv.at[l, n], sem_part.at[l, n, 1])
            summed = part_send[l, n, dp_me].astype(f32)
            for k in range(n_dp - 1):
                summed = summed + part_recv[l, n, k].astype(f32)
            summed = (inverse * summed).astype(bf16).astype(f32)
            drive = summed[:, 0:width]
            gate = summed[:, width:]
            for c in range(tiles):
                tile = n * tiles + c
                g0 = tile * per_tile
                channels = slice(tile * LANES, (tile + 1) * LANES)
                spread = jnp.concatenate(
                    [
                        jnp.where(
                            own_group,
                            jnp.broadcast_to(
                                drive[r : r + 1, c * LANES : (c + 1) * LANES], (per_tile, LANES)
                            ),
                            0.0,
                        )
                        for r in range(own_rows)
                    ],
                    axis=0,
                ).astype(bf16)
                raw = jnp.dot(spread, v_imap[l, channels, :], preferred_element_type=f32)
                a_r, a_i, c_r, c_i = (coef[l, i, g0 : g0 + per_tile, :] for i in range(4))
                history = []
                for s in range(own_seqs):
                    h = v_state[l, s, g0 : g0 + per_tile, :]
                    for t in range(new):
                        r0 = (s * new + t) * per_tile
                        u = raw[r0 : r0 + per_tile]
                        pushed = c_r * u + c_i * pltpu.roll(u, half, 1)
                        after = a_r * h + a_i * pltpu.roll(h, half, 1) + pushed
                        h = jnp.where(t < lens[s], after, h)
                        history.append(h * sign)
                    v_state[l, s, g0 : g0 + per_tile, :] = h
                stacked = jnp.concatenate(history, axis=0).astype(bf16)
                read = lax.dot_general(
                    stacked,
                    v_rmap[l, channels, :],
                    (((1,), (1,)), ((), ())),
                    preferred_element_type=f32,
                )
                for r in range(own_rows):
                    kept = jnp.where(own_group, read[r * per_tile : (r + 1) * per_tile], 0.0)
                    read_rows[r : r + 1, c * LANES : (c + 1) * LANES] = jnp.sum(
                        kept, axis=0, keepdims=True
                    )
            response = read_rows[...] + skip_row[:, n * width : (n + 1) * width] * drive
            branch = jax.nn.gelu(response) * (gate * jax.nn.sigmoid(gate)) * alive
            branch_all[l, n, dp_me] = branch.astype(bf16)
            for peer in dp_peers:
                push(
                    "dp",
                    peer,
                    branch_all.at[l, n, dp_me],
                    branch_all.at[l, n, dp_me],
                    sem_branch.at[l, n],
                )
            sends.append((branch_all.at[l, n, pl.ds(0, n_dp - 1)], sem_branch.at[l, n, 0]))
        saved = local(v_state.at[l], state_out.at[l], sem_out.at[l])

        projected = jnp.zeros((rows, features), f32)
        for n in range(CHUNKS):
            fetch["out", l, n].wait()
            settle(branch_all.at[l, n, pl.ds(0, n_dp - 1)], sem_branch.at[l, n, 1])
            for j in range(n_dp):
                b_rows[j * own_rows : (j + 1) * own_rows, :] = branch_all[l, n, j].astype(f32)
            projected = projected + jnp.dot(
                b_rows[...].astype(bf16), v_out[l, n], preferred_element_type=f32
            )
        if l < layers - 1:
            tp_all[l, tp_me] = projected.astype(bf16)
            for peer in tp_peers:
                push("tp", peer, tp_all.at[l, tp_me], tp_all.at[l, tp_me], sem_tp.at[l])
            sends.append((tp_all.at[l, pl.ds(0, n_tp - 1)], sem_tp.at[l, 0]))
            settle(tp_all.at[l, pl.ds(0, n_tp - 1)], sem_tp.at[l, 1])
            added = tp_all[l, 0].astype(f32)
            for j in range(1, n_tp):
                added = added + tp_all[l, j].astype(f32)
            x = (x + added).astype(bf16).astype(f32)
        else:
            for j in range(n_tp):
                block = slice(j * block_rows, (j + 1) * block_rows)
                rs_send[j] = projected[block].astype(bf16)
                x_recv[j] = x[block].astype(bf16)
            for k, peer in enumerate(tp_peers):
                push("tp", peer, rs_send.at[peer], rs_recv.at[k], sem_rs)
            sends.append((rs_recv, sem_rs.at[0]))
            base = x_recv[tp_me].astype(f32)
            added = rs_send[tp_me].astype(f32)
            settle(rs_recv, sem_rs.at[1])
            for k in range(n_tp - 1):
                added = added + rs_recv[k].astype(f32)
            v_mixed[...] = (base + added).astype(bf16)
            final = local(v_mixed, mixed_out, sem_out.at[layers])
        if l == 0:
            first_saved = [saved]
        else:
            first_saved.append(saved)
        if l == 0:
            settle(*sends.pop(0))
    for ref, sem in sends:
        settle(ref, sem)
    for copy in first_saved:
        copy.wait()
    final.wait()


def body(
    n_tp,
    n_dp,
    tokens,
    lengths,
    norm_gain,
    input_weight,
    gate_weight,
    decay_rate,
    frequency,
    log_step,
    input_map,
    readout_map,
    skip_weight,
    out_weight,
    state,
):
    layers, own_seqs, groups, state_width = state.shape
    block_seqs, new, features = tokens.shape
    inner = input_weight.shape[2]
    width = inner // CHUNKS
    block_rows = block_seqs * new
    rows = lengths.shape[0] * new
    own_rows = own_seqs * new
    any_spec = pl.BlockSpec(memory_space=pl.ANY)
    dma = pltpu.SemaphoreType.DMA
    mixed, new_state = pl.pallas_call(
        functools.partial(kernel, n_tp, n_dp),
        out_shape=(
            jax.ShapeDtypeStruct((block_rows, features), bf16),
            jax.ShapeDtypeStruct(state.shape, f32),
        ),
        in_specs=[pl.BlockSpec(memory_space=pltpu.SMEM)] + [any_spec] * 12,
        out_specs=(any_spec, any_spec),
        scratch_shapes=[
            pltpu.VMEM((layers, features), f32),
            pltpu.VMEM((layers, CHUNKS, features, width), bf16),
            pltpu.VMEM((layers, CHUNKS, features, width), bf16),
            pltpu.VMEM(decay_rate.shape, f32),
            pltpu.VMEM(frequency.shape, f32),
            pltpu.VMEM(log_step.shape, f32),
            pltpu.VMEM((layers, inner, state_width), bf16),
            pltpu.VMEM((layers, inner, state_width), bf16),
            pltpu.VMEM((layers, inner), bf16),
            pltpu.VMEM((layers, CHUNKS, width, features), bf16),
            pltpu.VMEM(state.shape, f32),
            pltpu.VMEM((block_rows, features), bf16),
            pltpu.VMEM((n_tp, block_rows, features), bf16),
            pltpu.VMEM((rows, features), f32),
            pltpu.VMEM((layers, n_dp, own_rows, LANES), f32),
            pltpu.VMEM((layers, n_dp - 1, own_rows, LANES), f32),
            pltpu.VMEM((layers, CHUNKS, n_dp, own_rows, 2 * width), bf16),
            pltpu.VMEM((layers, CHUNKS, n_dp - 1, own_rows, 2 * width), bf16),
            pltpu.VMEM((layers, CHUNKS, n_dp, own_rows, width), bf16),
            pltpu.VMEM((rows, width), f32),
            pltpu.VMEM((own_rows, width), f32),
            pltpu.VMEM((layers, n_tp, rows, features), bf16),
            pltpu.VMEM((n_tp, block_rows, features), bf16),
            pltpu.VMEM((n_tp - 1, block_rows, features), bf16),
            pltpu.VMEM((layers, 4, groups, state_width), f32),
            dma((7,)),
            dma((layers, CHUNKS, 4)),
            dma((layers + 1,)),
            dma((2,)),
            dma((layers, 2)),
            dma((layers, CHUNKS, 2)),
            dma((layers, CHUNKS, 2)),
            dma((layers, 2)),
            dma((2,)),
        ],
        compiler_params=pltpu.CompilerParams(
            collective_id=0, has_side_effects=True, vmem_limit_bytes=60 * 1024 * 1024
        ),
    )(
        lengths,
        tokens.reshape(block_rows, features),
        norm_gain,
        input_weight,
        gate_weight,
        decay_rate,
        frequency,
        log_step,
        input_map.reshape(layers, inner, state_width),
        readout_map.reshape(layers, inner, state_width),
        skip_weight,
        out_weight,
        state,
    )
    return mixed.reshape(tokens.shape), new_state


def solution(mesh):
    return jax.shard_map(
        functools.partial(body, mesh.shape["tp"], mesh.shape["dp"]),
        mesh=mesh,
        in_specs=(
            P(("grp", "tp"), None, "dp"),
            P("grp"),
            P(None, "dp"),
            P(None, "dp", "tp"),
            P(None, "dp", "tp"),
            P(None, "tp", None),
            P(None, "tp", None),
            P(None, "tp"),
            P(None, "tp", None, None),
            P(None, "tp", None, None),
            P(None, "tp"),
            P(None, "tp", "dp"),
            P(None, ("grp", "dp"), "tp", None),
        ),
        out_specs=(P(("grp", "tp"), None, "dp"), P(None, ("grp", "dp"), "tp", None)),
        check_vma=False,
    )
```

time: 200 us -> 51.7 us (0.26)
  blocking collectives: 88.4 us -> 0 us
  waiting for transfers between devices: 46.7 us -> 0 us
  Pallas kernels: 0 us -> 44.7 us
  matrix products: 26.6 us -> 0 us
  between operations: 18.3 us -> 0.64 us
  other arithmetic: 11.3 us -> 0 us
    unnamed x4 -> x0, waiting for transfers between devices: 46.7 us -> none
    pallas_call x0 -> x1, Pallas kernels: none -> 44.7 us  [body(): pl.pallas_call(functools.partial(kernel, n_tp, n_dp), out_shape=(jax.Shap...]
    all_gather x4 -> x0, blocking collectives: 38.8 us -> none  [the longest x2 28.3 us: body(): gathered = lax.all_gather(own_block, 'tp', axis=0, tiled=True)]
    unnamed x2 -> x0, blocking collectives: 38.1 us -> none
    dot_general x10 -> x0, matrix products: 26.6 us -> none  [the longest x2 6.96 us: body(): jnp.dot(scaled, gate_weight[layer_index], preferred_element_type=jnp.floa...]
    psum x2 -> x0, blocking collectives: 11.5 us -> none  [body(): total_squares = lax.psum(partial_squares, 'dp')]
    unnamed x33 -> x4, local copies, waits for them, and re-layouts: 2.22 us -> 6.05 us
    unnamed x3 -> x0, other arithmetic: 2.6 us -> none
  transfers between devices with their start and end apart: 2 -> 0, of which waited for: 2 -> 0; matrix products, arithmetic and copies ran while one was open for 3% -> 0% of each run, Pallas kernels for 0% -> 0%
where the time goes in v1:
time: 51.7 us; the launch traced here: 51.4 us
  Pallas kernels  44.7 us (86%)
  local copies, waits for them, and re-layouts  6.05 us (12%)
  between operations  0.64 us (1%)
    pallas_call x1, Pallas kernels, body(): pl.pallas_call(functools.partial(kernel, n_tp, n_dp), out_shape=(jax.Shap...  44.7 us
    unnamed x4, local copies, waits for them, and re-layouts  6.05 us

profile of v1, /device:TPU:0, one launch (start us, length us, event | category | flops | bytes accessed | tf_op | source)
XLA Modules:
  0.0 51.4 jit_solution(8171404328035633223)
XLA Ops:
  0.6 1.6 %copy.15.decay_rate = f32[2,128,64]{2,1,0:T(8,128)} copy(f32[2,128,64]{1,2,0:T(8,128)} %param.18) | data formatting | bytes 131072 | tf_op args[5]
  2.2 1.6 %copy.16.frequency = f32[2,128,64]{2,1,0:T(8,128)} copy(f32[2,128,64]{1,2,0:T(8,128)} %param.19) | data formatting | bytes 131072 | tf_op args[6]
  3.8 44.7 %shard_map.140 = (bf16[4,1024]{1,0:T(4,128)(2,1)}, f32[2,1,128,128]{3,2,1,0:T(8,128)}) custom-call(s32[4]{0:T(128)} %lengths.1, bf16[4,1024]{1,0:T(4,128)(2,1)} %bitcast.6, f32[2,1024]{1,0:T(2,128)} %norm_gain.1, bf16[2,1024,2048]{2,1,0:T(8,128)(2,1)} %input_weight.1, bf16[2,1024,2048]{2,1,0:T(8,128)(2,1)} %gate_weight.1, f32[2,128,64]{2,1,0:T(8,128)} %copy.15.decay_rate, ...), custom_call_target="tpu_custom_call" | custom-call | tf_op jit(solution)/shard_map/pallas_call | solution.py:353
  48.5 1.3 %copy.19 = bf16[1,4,1024]{2,1,0:T(4,128)(2,1)} copy(bf16[1,4,1024]{2,1,0:T(4,128)(2,1)} %bitcast.7) | data formatting | bytes 16384
  49.8 1.6 %copy.20 = f32[2,1,128,128]{3,2,1,0:T(8,128)} copy(f32[2,1,128,128]{3,2,1,0:T(8,128)} %get-tuple-element.9) | data formatting | bytes 262144

commit v2 on v1

--- a/solution.py
+++ b/solution.py
@@ -9,8 +9,14 @@
 
 D = 4096
 S5_IN = 16
-CHUNKS = 4
+CHUNKS = 2
 LANES = 128
+PLAN = {
+    "entry": (("proj", 0),),
+    "x0": (("map", 0), ("out", 0)),
+    "branch0": (("proj", 1), ("map", 1)),
+    "out0": (("out", 1),),
+}
 
 epsilon = 1e-06
 f32, bf16 = jnp.float32, jnp.bfloat16
@@ -59,6 +65,7 @@
     rs_send,
     rs_recv,
     coef,
+    lens_ref,
     sem_small,
     sem_w,
     sem_out,
@@ -99,23 +106,41 @@
                 (log_step, v_step),
                 (skip_weight, v_skip),
                 (state, v_state),
+                (lengths, lens_ref),
             )
         )
     ]
     fetch = {}
-    for l in range(layers):
-        for n in range(CHUNKS):
-            cols = pl.ds(n * width, width)
-            fetch["in", l, n] = local(input_weight.at[l, :, cols], v_in.at[l, n], sem_w.at[l, n, 0])
-            fetch["gate", l, n] = local(gate_weight.at[l, :, cols], v_gate.at[l, n], sem_w.at[l, n, 1])
-        fetch["imap", l] = local(input_map.at[l], v_imap.at[l], sem_w.at[l, 0, 3])
-        fetch["rmap", l] = local(readout_map.at[l], v_rmap.at[l], sem_w.at[l, 1, 3])
-        for n in range(CHUNKS):
-            cols = pl.ds(n * width, width)
-            fetch["out", l, n] = local(out_weight.at[l, cols, :], v_out.at[l, n], sem_w.at[l, n, 2])
+
+    def load(point):
+        for kind, l in PLAN.get(point, ()):
+            for n in range(CHUNKS):
+                cols = pl.ds(n * width, width)
+                if kind == "proj":
+                    fetch["in", l, n] = local(
+                        input_weight.at[l, :, cols], v_in.at[l, n], sem_w.at[l, n, 0]
+                    )
+                    fetch["gate", l, n] = local(
+                        gate_weight.at[l, :, cols], v_gate.at[l, n], sem_w.at[l, n, 1]
+                    )
+                elif kind == "out":
+                    fetch["out", l, n] = local(
+                        out_weight.at[l, cols, :], v_out.at[l, n], sem_w.at[l, n, 2]
+                    )
+                elif n == 0:
+                    fetch["imap", l] = local(input_map.at[l], v_imap.at[l], sem_w.at[l, 0, 3])
+                    fetch["rmap", l] = local(readout_map.at[l], v_rmap.at[l], sem_w.at[l, 1, 3])
+
+    load("entry")
 
     barrier = pltpu.get_barrier_semaphore()
-    tp_peers = [lax.rem(tp_me + k, n_tp) for k in range(1, n_tp)]
+    upper = tp_me // max(n_tp // 2, 1)
+    tp_peers = []
+    for k in range(n_tp - 1):
+        top = n_tp - 1 - k
+        low = top - 1 + (top + n_tp - tp_me - 1) // n_tp
+        high = k + (k + n_tp - tp_me) // n_tp
+        tp_peers.append(low + upper * (high - low))
     dp_peers = [lax.rem(dp_me + k, n_dp) for k in range(1, n_dp)]
     for peer in tp_peers:
         pl.semaphore_signal(
@@ -128,6 +153,7 @@
     pl.semaphore_wait(barrier, n_tp + n_dp - 2)
 
     sends = []
+    saves = []
 
     def push(axis, peer, src, dst, sems):
         copy = pltpu.make_async_remote_copy(
@@ -148,10 +174,11 @@
         push("tp", peer, x_recv.at[tp_me], x_recv.at[tp_me], sem_x)
     sends.append((x_recv.at[pl.ds(0, n_tp - 1)], sem_x.at[0]))
 
+    load("sent")
     for copy in small[1:]:
         copy.wait()
     for l in range(layers):
-        step = jnp.exp(jnp.broadcast_to(v_step[l : l + 1, :], (LANES, groups)).T)[:, :half]
+        step = jnp.exp(v_step[l : l + 1, :])
         rate = v_decay[l]
         freq = v_freq[l]
         magnitude = jnp.exp(-rate * step)
@@ -162,13 +189,13 @@
         cr = (-(ar - 1.0) * rate + ai * freq) / den
         ci = (-ai * rate - (ar - 1.0) * freq) / den
         for i, (low, high) in enumerate(((ar, ar), (-ai, ai), (cr, cr), (-ci, ci))):
-            coef[l, i, :, 0:half] = low
-            coef[l, i, :, half:] = high
+            coef[l, i] = jnp.concatenate([low, high], axis=0).T
 
     settle(x_recv.at[pl.ds(0, n_tp - 1)], sem_x.at[1])
     for j in range(n_tp):
         x_all[j * block_rows : (j + 1) * block_rows, :] = x_recv[j].astype(f32)
     x = x_all[...]
+    load("x0")
 
     lane = lax.broadcasted_iota(jnp.int32, (per_tile, LANES), 1)
     sub = lax.broadcasted_iota(jnp.int32, (per_tile, LANES), 0)
@@ -176,7 +203,7 @@
     sign = jnp.where(
         lax.broadcasted_iota(jnp.int32, (1, state_width), 1) < half, jnp.float32(1), jnp.float32(-1)
     )
-    lens = [lengths[dp_me * own_seqs + s] for s in range(own_seqs)]
+    lens = [lens_ref[dp_me * own_seqs + s] for s in range(own_seqs)]
     row_id = lax.broadcasted_iota(jnp.int32, (own_rows, 1), 0)
     alive = jnp.zeros((own_rows, 1), f32)
     for s in range(own_seqs):
@@ -205,6 +232,7 @@
                 push("dp", peer, part_send.at[l, n, peer], part_recv.at[l, n, k], sem_part.at[l, n])
             sends.append((part_recv.at[l, n], sem_part.at[l, n, 0]))
 
+        load(f"proj{l}")
         fetch["imap", l].wait()
         fetch["rmap", l].wait()
         settle(sq_recv.at[l], sem_sq.at[l, 1])
@@ -221,45 +249,54 @@
             summed = (inverse * summed).astype(bf16).astype(f32)
             drive = summed[:, 0:width]
             gate = summed[:, width:]
+            pieces = []
+            for c in range(tiles):
+                for r in range(own_rows):
+                    spread = jnp.broadcast_to(
+                        drive[r : r + 1, c * LANES : (c + 1) * LANES], (per_tile, LANES)
+                    )
+                    pieces.append(jnp.where(own_group, spread, 0.0))
+            raws = []
             for c in range(tiles):
                 tile = n * tiles + c
-                g0 = tile * per_tile
-                channels = slice(tile * LANES, (tile + 1) * LANES)
-                spread = jnp.concatenate(
-                    [
-                        jnp.where(
-                            own_group,
-                            jnp.broadcast_to(
-                                drive[r : r + 1, c * LANES : (c + 1) * LANES], (per_tile, LANES)
-                            ),
-                            0.0,
-                        )
-                        for r in range(own_rows)
-                    ],
-                    axis=0,
+                spread = jnp.concatenate(pieces[c * own_rows : (c + 1) * own_rows], axis=0)
+                raws.append(
+                    jnp.dot(
+                        spread.astype(bf16),
+                        v_imap[l, tile * LANES : (tile + 1) * LANES, :],
+                        preferred_element_type=f32,
+                    )
+                )
+            here = slice(n * tiles * per_tile, (n + 1) * tiles * per_tile)
+            a_r, a_i, c_r, c_i = (coef[l, i, here, :] for i in range(4))
+            history = []
+            for s in range(own_seqs):
+                h = v_state[l, s, here, :]
+                for t in range(new):
+                    r0 = (s * new + t) * per_tile
+                    u = jnp.concatenate([raw[r0 : r0 + per_tile] for raw in raws], axis=0)
+                    pushed = c_r * u + c_i * pltpu.roll(u, half, 1)
+                    after = a_r * h + a_i * pltpu.roll(h, half, 1) + pushed
+                    h = jnp.where(t < lens[s], after, h)
+                    history.append((h * sign).astype(f32))
+                state_out[l, s, here, :] = h
+            reads = []
+            for c in range(tiles):
+                tile = n * tiles + c
+                stacked = jnp.concatenate(
+                    [h[c * per_tile : (c + 1) * per_tile] for h in history], axis=0
                 ).astype(bf16)
-                raw = jnp.dot(spread, v_imap[l, channels, :], preferred_element_type=f32)
-                a_r, a_i, c_r, c_i = (coef[l, i, g0 : g0 + per_tile, :] for i in range(4))
-                history = []
-                for s in range(own_seqs):
-                    h = v_state[l, s, g0 : g0 + per_tile, :]
-                    for t in range(new):
-                        r0 = (s * new + t) * per_tile
-                        u = raw[r0 : r0 + per_tile]
-                        pushed = c_r * u + c_i * pltpu.roll(u, half, 1)
-                        after = a_r * h + a_i * pltpu.roll(h, half, 1) + pushed
-                        h = jnp.where(t < lens[s], after, h)
-                        history.append(h * sign)
-                    v_state[l, s, g0 : g0 + per_tile, :] = h
-                stacked = jnp.concatenate(history, axis=0).astype(bf16)
-                read = lax.dot_general(
-                    stacked,
-                    v_rmap[l, channels, :],
-                    (((1,), (1,)), ((), ())),
-                    preferred_element_type=f32,
+                reads.append(
+                    lax.dot_general(
+                        stacked,
+                        v_rmap[l, tile * LANES : (tile + 1) * LANES, :],
+                        (((1,), (1,)), ((), ())),
+                        preferred_element_type=f32,
+                    )
                 )
+            for c in range(tiles):
                 for r in range(own_rows):
-                    kept = jnp.where(own_group, read[r * per_tile : (r + 1) * per_tile], 0.0)
+                    kept = jnp.where(own_group, reads[c][r * per_tile : (r + 1) * per_tile], 0.0)
                     read_rows[r : r + 1, c * LANES : (c + 1) * LANES] = jnp.sum(
                         kept, axis=0, keepdims=True
                     )
@@ -275,7 +312,7 @@
                     sem_branch.at[l, n],
                 )
             sends.append((branch_all.at[l, n, pl.ds(0, n_dp - 1)], sem_branch.at[l, n, 0]))
-        saved = local(v_state.at[l], state_out.at[l], sem_out.at[l])
+        load(f"branch{l}")
 
         projected = jnp.zeros((rows, features), f32)
         for n in range(CHUNKS):
@@ -291,6 +328,7 @@
             for peer in tp_peers:
                 push("tp", peer, tp_all.at[l, tp_me], tp_all.at[l, tp_me], sem_tp.at[l])
             sends.append((tp_all.at[l, pl.ds(0, n_tp - 1)], sem_tp.at[l, 0]))
+            load(f"out{l}")
             settle(tp_all.at[l, pl.ds(0, n_tp - 1)], sem_tp.at[l, 1])
             added = tp_all[l, 0].astype(f32)
             for j in range(1, n_tp):
@@ -301,27 +339,22 @@
                 block = slice(j * block_rows, (j + 1) * block_rows)
                 rs_send[j] = projected[block].astype(bf16)
                 x_recv[j] = x[block].astype(bf16)
-            for k, peer in enumerate(tp_peers):
-                push("tp", peer, rs_send.at[peer], rs_recv.at[k], sem_rs)
-            sends.append((rs_recv, sem_rs.at[0]))
+            for peer in tp_peers:
+                slot = lax.rem(tp_me - peer + n_tp, n_tp) - 1
+                push("tp", peer, rs_send.at[peer], rs_recv.at[slot], sem_rs)
+            for ref, sem in sends:
+                settle(ref, sem)
+            for copy in saves:
+                copy.wait()
             base = x_recv[tp_me].astype(f32)
             added = rs_send[tp_me].astype(f32)
             settle(rs_recv, sem_rs.at[1])
             for k in range(n_tp - 1):
                 added = added + rs_recv[k].astype(f32)
-            v_mixed[...] = (base + added).astype(bf16)
-            final = local(v_mixed, mixed_out, sem_out.at[layers])
-        if l == 0:
-            first_saved = [saved]
-        else:
-            first_saved.append(saved)
+            mixed_out[...] = (base + added).astype(bf16)
         if l == 0:
             settle(*sends.pop(0))
-    for ref, sem in sends:
-        settle(ref, sem)
-    for copy in first_saved:
-        copy.wait()
-    final.wait()
+    settle(rs_recv, sem_rs.at[0])
 
 
 def body(
@@ -353,17 +386,17 @@
     mixed, new_state = pl.pallas_call(
         functools.partial(kernel, n_tp, n_dp),
         out_shape=(
-            jax.ShapeDtypeStruct((block_rows, features), bf16),
-            jax.ShapeDtypeStruct(state.shape, f32),
+            pltpu.VMEM((block_rows, features), bf16),
+            pltpu.VMEM(state.shape, f32),
         ),
-        in_specs=[pl.BlockSpec(memory_space=pltpu.SMEM)] + [any_spec] * 12,
-        out_specs=(any_spec, any_spec),
+        in_specs=[any_spec] * 13,
+        out_specs=(pl.BlockSpec(memory_space=pltpu.VMEM),) * 2,
         scratch_shapes=[
             pltpu.VMEM((layers, features), f32),
             pltpu.VMEM((layers, CHUNKS, features, width), bf16),
             pltpu.VMEM((layers, CHUNKS, features, width), bf16),
-            pltpu.VMEM(decay_rate.shape, f32),
-            pltpu.VMEM(frequency.shape, f32),
+            pltpu.VMEM((layers, state_width // 2, groups), f32),
+            pltpu.VMEM((layers, state_width // 2, groups), f32),
             pltpu.VMEM(log_step.shape, f32),
             pltpu.VMEM((layers, inner, state_width), bf16),
             pltpu.VMEM((layers, inner, state_width), bf16),
@@ -384,7 +417,8 @@
             pltpu.VMEM((n_tp, block_rows, features), bf16),
             pltpu.VMEM((n_tp - 1, block_rows, features), bf16),
             pltpu.VMEM((layers, 4, groups, state_width), f32),
-            dma((7,)),
+            pltpu.SMEM(lengths.shape, jnp.int32),
+            dma((8,)),
             dma((layers, CHUNKS, 4)),
             dma((layers + 1,)),
             dma((2,)),
@@ -403,8 +437,8 @@
         norm_gain,
         input_weight,
         gate_weight,
-        decay_rate,
-        frequency,
+        jnp.swapaxes(decay_rate, 1, 2),
+        jnp.swapaxes(frequency, 1, 2),
         log_step,
         input_map.reshape(layers, inner, state_width),
         readout_map.reshape(layers, inner, state_width),

time: 51.7 us -> 35.4 us (0.68)
  Pallas kernels: 44.7 us -> 33.4 us
  local copies, waits for them, and re-layouts: 6.05 us -> 1.26 us
    pallas_call x1, Pallas kernels: 44.7 us -> 33.4 us  [body(): pl.pallas_call(functools.partial(kernel, n_tp, n_dp), out_shape=(pltpu.VM...]
    unnamed x4 -> x2, local copies, waits for them, and re-layouts: 6.05 us -> 1.26 us
where the time goes in v2:
time: 35.4 us; the launch traced here: 35.3 us
  Pallas kernels  33.4 us (94%)
  local copies, waits for them, and re-layouts  1.26 us (4%)
  between operations  0.64 us (2%)
    pallas_call x1, Pallas kernels, body(): pl.pallas_call(functools.partial(kernel, n_tp, n_dp), out_shape=(pltpu.VM...  33.4 us
    unnamed x2, local copies, waits for them, and re-layouts  1.26 us

profile of v2, /device:TPU:0, one launch (start us, length us, event | category | flops | bytes accessed | tf_op | source)
XLA Modules:
  0.0 35.3 jit_solution(9719143574323110149)
XLA Ops:
  0.6 33.4 %shard_map.140 = (bf16[4,1024]{1,0:T(4,128)(2,1)S(1)}, f32[2,1,128,128]{3,2,1,0:T(8,128)S(1)}) custom-call(s32[4]{0:T(128)} %lengths.1, bf16[4,1024]{1,0:T(4,128)(2,1)} %bitcast.11, f32[2,1024]{1,0:T(2,128)} %norm_gain.1, bf16[2,1024,2048]{2,1,0:T(8,128)(2,1)} %input_weight.1, bf16[2,1024,2048]{2,1,0:T(8,128)(2,1)} %gate_weight.1, f32[2,64,128]{2,1,0:T(8,128)} %bitcast.9, ...), custom_call_target="tpu_custom_call" | custom-call | tf_op jit(solution)/shard_map/pallas_call | solution.py:386
  34.0 0.6 %copy.17 = bf16[1,4,1024]{2,1,0:T(4,128)(2,1)} copy(bf16[1,4,1024]{2,1,0:T(4,128)(2,1)S(1)} %bitcast.6) | data formatting | bytes 16384
  34.6 0.7 %copy.18 = f32[2,1,128,128]{3,2,1,0:T(8,128)} copy(f32[2,1,128,128]{3,2,1,0:T(8,128)S(1)} %get-tuple-element.7) | data formatting | bytes 262144
